TPU v7x, 32 devices: a whole 2x2x4 slice. The times are simulated.
32 devices in a mesh: rep: 2 (over x), fs: 8 (over z, y), tp: 2 (over core).
Axes of the slice: x: 2, y: 2, z: 4, core: 2. Of those that a mesh axis runs over, the one named last changes fastest.
Arguments:
- pre_gate: bfloat16 [12288, 4096], P(('rep', 'fs'), 'tp'), may hold values from -6 to 6
- pre_linear: bfloat16 [12288, 4096], P(('rep', 'fs'), 'tp'), may hold values from -6 to 6
- taps_gate: float32 [3, 4096], P(None, 'tp'), may hold values from -3.5 to 3.5
- taps_linear: float32 [3, 4096], P(None, 'tp'), may hold values from -3.5 to 3.5
- bias_gate: float32 [4096], P('tp'), may hold values from -3 to 3
- bias_linear: float32 [4096], P('tp'), may hold values from -3 to 3
- down_weight: bfloat16 [4096, 2048], P('tp', 'fs'), may hold values from -0.09375 to 0.09375
- out_grad: bfloat16 [12288, 2048], P(('rep', 'fs')), may hold values from -8 to 8
Outputs:
- grad_gate: bfloat16 [12288, 4096], P(('rep', 'fs'), 'tp')
- grad_linear: bfloat16 [12288, 4096], P(('rep', 'fs'), 'tp')
- grad_taps_gate: float32 [3, 4096], P(None, 'tp')
- grad_taps_linear: float32 [3, 4096], P(None, 'tp')
- grad_bias_gate: float32 [4096], P('tp')
- grad_bias_linear: float32 [4096], P('tp')
- grad_down: float32 [4096, 2048], P('tp', 'fs')
- row_norms: float32 [4096], P('tp')
All inputs are finite; a program needn't handle non-finite values.
Results may differ from a plain program's by a relative error of at most 0.0031.
Values may be sent and summed in bfloat16 or wider, within the bound.
No kernel may reach another device: no remote copies, remote signals or barrier semaphores. Data moves between devices by JAX's collectives and lax.ppermute only.
A program may use at most 128 MiB of HBM per device.

v0:
```python
import jax
import jax.numpy as jnp
from jax import lax
from jax.sharding import PartitionSpec as P


def convolve(values, taps, bias):
    length = values.shape[0]
    padded = jnp.pad(values, ((2, 0), (0, 0)))
    return (
        taps[0] * padded[0:length]
        + taps[1] * padded[1 : length + 1]
        + taps[2] * padded[2 : length + 2]
        + bias
    )


def convolve_back(grads, taps):
    length = grads.shape[0]
    padded = jnp.pad(grads, ((0, 2), (0, 0)))
    return (
        taps[0] * padded[2 : length + 2]
        + taps[1] * padded[1 : length + 1]
        + taps[2] * padded[0:length]
    )


def tap_grads(grads, values):
    length = values.shape[0]
    padded = jnp.pad(values, ((2, 0), (0, 0)))
    return jnp.stack([jnp.sum(grads * padded[j : j + length], axis=0) for j in range(3)])


def local(
    pre_gate, pre_linear, taps_gate, taps_linear, bias_gate, bias_linear, down_weight, out_grad
):
    gate_in = pre_gate.astype(jnp.float32)
    linear_in = pre_linear.astype(jnp.float32)
    gate_pre = convolve(gate_in, taps_gate, bias_gate)
    linear_pre = convolve(linear_in, taps_linear, bias_linear)
    sigma = jax.nn.sigmoid(gate_pre)
    silu_val = gate_pre * sigma
    hidden = (silu_val * linear_pre).astype(jnp.bfloat16)
    columns = out_grad
    grad_hidden = lax.dot_general(
        columns,
        lax.all_gather(down_weight, "fs", axis=1, tiled=True),
        (((1,), (1,)), ((), ())),
        preferred_element_type=jnp.float32,
    )
    grad_gate_pre = grad_hidden * linear_pre * sigma * (1.0 + gate_pre * (1.0 - sigma))
    grad_linear_pre = grad_hidden * silu_val
    grad_gate = convolve_back(grad_gate_pre, taps_gate).astype(jnp.bfloat16)
    grad_linear = convolve_back(grad_linear_pre, taps_linear).astype(jnp.bfloat16)
    conv_parts = (
        tap_grads(grad_gate_pre, gate_in),
        tap_grads(grad_linear_pre, linear_in),
        jnp.sum(grad_gate_pre, axis=0),
        jnp.sum(grad_linear_pre, axis=0),
    )
    grad_taps_gate, grad_taps_linear, grad_bias_gate, grad_bias_linear = lax.psum(
        (conv_parts[0], conv_parts[1], conv_parts[2], conv_parts[3]), ("rep", "fs")
    )
    columns = out_grad
    partial_grad = lax.psum_scatter(
        lax.dot_general(
            columns, hidden, (((0,), (0,)), ((), ())), preferred_element_type=jnp.float32
        ),
        "fs",
        scatter_dimension=0,
        tiled=True,
    )
    summed = lax.psum(partial_grad, "rep")
    grad_down = summed.T
    row_norms = lax.psum(jnp.sum(grad_down * grad_down, axis=1), "fs")
    return (
        grad_gate,
        grad_linear,
        grad_taps_gate,
        grad_taps_linear,
        grad_bias_gate,
        grad_bias_linear,
        grad_down,
        row_norms,
    )


def solution(mesh):
    in_specs = (
        P(("rep", "fs"), "tp"),
        P(("rep", "fs"), "tp"),
        P(None, "tp"),
        P(None, "tp"),
        P("tp"),
        P("tp"),
        P("tp", "fs"),
        P(("rep", "fs"), None),
    )
    out_specs = (
        P(("rep", "fs"), "tp"),
        P(("rep", "fs"), "tp"),
        P(None, "tp"),
        P(None, "tp"),
        P("tp"),
        P("tp"),
        P("tp", "fs"),
        P("tp"),
    )
    return jax.shard_map(local, mesh=mesh, in_specs=in_specs, out_specs=out_specs, check_vma=False)
```

profile of v0, /device:TPU:0, one launch (start us, length us, event | category | flops | bytes accessed | tf_op | source)
XLA Modules:
  0.0 668.1 jit_solution(7865275278848254621)
XLA Ops:
  7.2 0.0 copy-start
  7.2 0.0 all-gather.2.cloned.1.call-start
  7.2 0.7 all-gather.2.cloned.1.call-update
  7.9 0.0 reduce-scatter.2.cloned.1.call-start
  8.0 0.0 copy-start.3
  8.0 5.6 convert_element_type.24
  13.5 0.0 copy-done.3
  13.5 0.0 copy-start.4
  13.5 0.0 copy-start.5
  13.5 0.0 copy-start.7
  13.5 3.4 convert_element_type.23
  17.0 0.0 copy-done.4
  17.0 0.0 copy-done.5
  17.0 120.7 %all-gather.2.cloned.1.call-done = bf16[2048,2048]{1,0:T(8,128)(2,1)} async-done(((bf16[2048,256]{1,0:T(8,128)(2,1)}), bf16[2048,2048]{1,0:T(8,128)(2,1)}) %all-gather.2.cloned.1.call-update) | async-done | bytes 8388624 | tf_op jit(solution)/shard_map/all_gather | solution.py:47
  137.7 0.0 copy-done
  137.7 0.0 copy-done.7
  137.7 0.0 copy-start.1
  137.7 0.0 copy-start.2
  137.7 0.0 copy-start.6
  137.8 25.9 %fusion.4 = (f32[2048]{0:T(1024)}, f32[2048]{0:T(1024)S(1)}, f32[2048]{0:T(1024)S(1)}, f32[2048]{0:T(1024)S(1)}, f32[768,2048]{1,0:T(8,128)}, /*index=5*/f32[768,2048]{1,0:T(8,128)}, f32[768,2048]{1,0:T(8,128)}) fusion(bf16[768,2048]{1,0:T(8,128)(2,1)} %param.9, f32[768,2048]{1,0:T(8,128)} %convert_element_type.23, f32[2048]{0:T(1024)S(1)} %copy-done.7, ...), kind=kOutput, calls=%fused_computation.24 | convolution fusion | flops 6472327168 | bytes 46202880 | tf_op jit(solution)/shard_map/dot_general | solution.py:45
  163.7 0.0 copy-done.1
  163.7 0.0 copy-done.2
  163.7 0.0 copy-done.6
  163.7 19.0 %fusion.5 = (f32[2048]{0:T(1024)}, f32[2048]{0:T(1024)S(1)}, f32[2048]{0:T(1024)S(1)}, f32[2048]{0:T(1024)S(1)}, f32[768,2048]{1,0:T(8,128)}, /*index=5*/f32[768,2048]{1,0:T(8,128)}, bf16[768,2048]{1,0:T(8,128)(2,1)}) fusion(bf16[768,2048]{1,0:T(8,128)(2,1)} %param.8, f32[768,2048]{1,0:T(8,128)S(1)} %copy-done.1, f32[768,2048]{1,0:T(8,128)} %get-tuple-element.25, ...), kind=kLoop, calls=%fused_computation.25 | loop fusion | flops 45604864 | bytes 50397184 | tf_op jit(solution)/shard_map/reduce_sum | solution.py:58
  182.7 15.2 %convolution_bitcast_fusion = f32[2048,2048]{0,1:T(8,128)} fusion(bf16[768,2048]{1,0:T(8,128)(2,1)S(1)} %copy-done, f32[768,2048]{1,0:T(8,128)} %get-tuple-element.27, f32[768,2048]{1,0:T(8,128)} %get-tuple-element.25), kind=kOutput, calls=%fused_computation | convolution fusion | flops 6451888128 | bytes 32505856 | tf_op jit(solution)/shard_map/dot_general | solution.py:66
  197.8 0.0 reduce-scatter.2.cloned.1.call-update
  197.9 0.0 all-reduce.8.cloned.1.call-start
  197.9 278.5 %reduce-scatter.2.cloned.1.call-done = f32[256,2048]{0,1:T(8,128)} async-done(((f32[2048,2048]{0,1:T(8,128)}), f32[256,2048]{0,1:T(8,128)}) %reduce-scatter.2.cloned.1.call-update) | async-done | bytes 2097168 | tf_op jit(solution)/shard_map/reduce_scatter | solution.py:65
  476.4 0.0 all-reduce.8.cloned.1.call-update
  476.5 0.0 all-reduce.10.cloned.1.call-start
  476.5 0.7 pad_maximum_fusion
  477.2 9.6 %add_convert_fusion.1 = bf16[768,2048]{1,0:T(8,128)(2,1)} fusion(f32[768,2048]{1,0:T(8,128)} %get-tuple-element.26, f32[2048]{0:T(1024)S(1)} %bitcast.28, f32[2048]{0:T(1024)S(1)} %bitcast.30, f32[2048]{0:T(1024)S(1)} %bitcast.26), kind=kLoop, calls=%fused_computation.9 | loop fusion | flops 9437184 | bytes 9461760 | tf_op jit(solution)/shard_map/convert_element_type | solution.py:53
  486.8 0.0 all-reduce.10.cloned.1.call-update
  486.8 54.0 %all-reduce.8.cloned.1.call-done = f32[2048,256]{1,0:T(8,128)} async-done(((f32[2048,256]{1,0:T(8,128)}), f32[2048,256]{1,0:T(8,128)}) %all-reduce.8.cloned.1.call-update) | async-done | bytes 2097168 | tf_op jit(solution)/shard_map/psum | solution.py:73
  540.8 1.9 multiply_reduce_fusion.6
  542.8 22.3 %psum.47 = f32[2048]{0:T(1024)} all-reduce(f32[2048]{0:T(1024)S(1)} %multiply_reduce_fusion.6), channel_id=1, replica_groups=mesh['rep'=2,'fs'=8,'tp'=2] {'fs'}, use_global_device_ids=true, to_apply=%region_15.16 | all-reduce | flops 2048 | bytes 16384 | tf_op jit(solution)/shard_map/psum | solution.py:75
  565.1 88.1 %all-reduce.10.cloned.1.call-done = (f32[3,2048]{1,0:T(4,128)}, f32[3,2048]{1,0:T(4,128)}, f32[2048]{0:T(1024)}, f32[2048]{0:T(1024)}) async-done(((f32[3,2048]{1,0:T(4,128)}, f32[3,2048]{1,0:T(4,128)}, f32[2048]{0:T(1024)}, f32[2048]{0:T(1024)}), (f32[3,2048]{1,0:T(4,128)}, f32[3,2048]{1,0:T(4,128)}, f32[2048]{0:T(1024)}, f32[2048]{0:T(1024)})) %all-reduce.10.cloned.1.call-update) | async-done | bytes 65552 | tf_op jit(solution)/shard_map/psum | solution.py:61
  653.2 1.4 copy.21
  654.6 1.4 copy.22
  655.9 1.3 copy.23
  657.2 1.3 copy.24
  658.5 3.0 copy.25
  (2 shorter events, 0.0 us)
Async XLA Ops:
  7.2 130.6 %copy-start = (bf16[768,2048]{1,0:T(8,128)(2,1)S(1)}, bf16[768,2048]{1,0:T(8,128)(2,1)}, u32[]{:S(2)}) copy-start(bf16[768,2048]{1,0:T(8,128)(2,1)} %param.15) | copy-start | bytes 9437188
  7.2 130.5 %all-gather.2.cloned.1.call-start = ((), (), s32[]{:S(2)}) async-start(), calls=%async_computation.1 | async-start | bytes 9437184 | tf_op jit(solution)/shard_map/all_gather | solution.py:47
  7.9 468.5 %reduce-scatter.2.cloned.1.call-start = ((), (), s32[]{:S(2)}) async-start(), calls=%async_computation.2 | async-start | bytes 18874368 | tf_op jit(solution)/shard_map/reduce_scatter | solution.py:65
  8.0 5.6 copy-start.3
  13.5 3.4 copy-start.4
  13.5 3.5 copy-start.5
  13.5 124.2 %copy-start.7 = (f32[2048]{0:T(1024)S(1)}, f32[2048]{0:T(1024)}, u32[]{:S(2)}) copy-start(f32[2048]{0:T(1024)} %param.12) | copy-start | bytes 24580
  137.7 25.9 %copy-start.1 = (f32[768,2048]{1,0:T(8,128)S(1)}, f32[768,2048]{1,0:T(8,128)}, u32[]{:S(2)}) copy-start(f32[768,2048]{1,0:T(8,128)} %convert_element_type.24) | copy-start | bytes 18874372
  137.7 25.9 %copy-start.2 = (f32[768,2048]{1,0:T(8,128)S(1)}, f32[768,2048]{1,0:T(8,128)}, u32[]{:S(2)}) copy-start(f32[768,2048]{1,0:T(8,128)} %convert_element_type.23) | copy-start | bytes 18874372
  137.7 25.9 %copy-start.6 = (f32[2048]{0:T(1024)S(1)}, f32[2048]{0:T(1024)}, u32[]{:S(2)}) copy-start(f32[2048]{0:T(1024)} %param.13) | copy-start | bytes 24580
  197.9 343.0 %all-reduce.8.cloned.1.call-start = ((), (), s32[]{:S(2)}) async-start(), calls=%async_computation.3 | async-start | bytes 4194304 | tf_op jit(solution)/shard_map/psum | solution.py:73
  476.5 176.7 %all-reduce.10.cloned.1.call-start = ((), (), s32[]{:S(2)}) async-start(), calls=%async_computation.4 | async-start | bytes 163840 | tf_op jit(solution)/shard_map/psum | solution.py:61
Sparse Core Ops, SparseCore 0:
  10.0 127.6 all-gather.1
  198.0 278.3 reduce-scatter.1
  478.7 62.0 all-reduce.7
  547.2 105.9 all-reduce.9
where the time goes:
time: 669 us; the launch traced here: 668 us
  waiting for transfers between devices  542 us (81%)
  matrix products  41.1 us (6%)
  other arithmetic  40.2 us (6%)
  blocking collectives  22.3 us (3%)
  between operations  13.8 us (2%)
  local copies, waits for them, and re-layouts  8.47 us (1%)
    reduce_scatter x1, waiting for transfers between devices, local(): lax.psum_scatter(lax.dot_general(columns, hidden, (((0,), (0,)), ((), ())...  279 us
    all_gather x1, waiting for transfers between devices, local(): lax.all_gather(down_weight, 'fs', axis=1, tiled=True)  121 us
    psum x1, waiting for transfers between devices, local(): lax.psum((conv_parts[0], conv_parts[1], conv_parts[2], conv_parts[3]), ('...  88.1 us
    psum x1, waiting for transfers between devices, local(): summed = lax.psum(partial_grad, 'rep')  54 us
    dot_general x1, matrix products, local(): lax.dot_general(columns, lax.all_gather(down_weight, 'fs', axis=1, tiled=...  25.9 us
    psum x1, blocking collectives, local(): row_norms = lax.psum(jnp.sum(grad_down * grad_down, axis=1), 'fs')  22.3 us
    reduce_sum x1, other arithmetic, local(): jnp.sum(grad_gate_pre, axis=0)  19 us
    dot_general x1, matrix products, local(): lax.dot_general(columns, hidden, (((0,), (0,)), ((), ())), preferred_elem...  15.2 us
  transfers between devices with their start and end apart: 4, of which 4 were waited for; matrix products, arithmetic and copies ran while one was open for 3% of the time, Pallas kernels for 0%

commit v1 on v0

--- a/solution.py
+++ b/solution.py
@@ -58,8 +58,16 @@
         jnp.sum(grad_gate_pre, axis=0),
         jnp.sum(grad_linear_pre, axis=0),
     )
-    grad_taps_gate, grad_taps_linear, grad_bias_gate, grad_bias_linear = lax.psum(
-        (conv_parts[0], conv_parts[1], conv_parts[2], conv_parts[3]), ("rep", "fs")
+
+    def run_rounds_here(x_local):
+        named_axis = "rep"
+        link_axis = "fs"
+        for k0 in (named_axis, link_axis):
+            x_local = lax.psum(x_local, axis_name=k0)
+        return x_local
+
+    grad_taps_gate, grad_taps_linear, grad_bias_gate, grad_bias_linear = run_rounds_here(
+        (conv_parts[0], conv_parts[1], conv_parts[2], conv_parts[3])
     )
     columns = out_grad
     partial_grad = lax.psum_scatter(

time: 669 us -> 658 us (0.984)
  blocking collectives: 22.3 us -> 0 us
  waiting for transfers between devices: 542 us -> 551 us
    psum x1 -> x0, blocking collectives: 22.3 us -> none  [local(): row_norms = lax.psum(jnp.sum(grad_down * grad_down, axis=1), 'fs')]
    psum x1, waiting for transfers between devices: 54 us -> 63.6 us  [local(): summed = lax.psum(partial_grad, 'rep')]
    psum x1 -> x2, waiting for transfers between devices: 88.1 us -> 87.8 us  [run_rounds_here(): x_local = lax.psum(x_local, axis_name=k0)]
  transfers between devices with their start and end apart: 4 -> 5, of which waited for: 4 -> 5; matrix products, arithmetic and copies ran while one was open for 3% -> 3% of each run, Pallas kernels for 0% -> 0%
where the time goes in v1:
time: 658 us; the launch traced here: 657 us
  waiting for transfers between devices  551 us (84%)
  matrix products  41.1 us (6%)
  other arithmetic  41 us (6%)
  between operations  13.8 us (2%)
  local copies, waits for them, and re-layouts  9.76 us (1%)
    reduce_scatter x1, waiting for transfers between devices, local(): lax.psum_scatter(lax.dot_general(columns, hidden, (((0,), (0,)), ((), ())...  279 us
    all_gather x1, waiting for transfers between devices, local(): lax.all_gather(down_weight, 'fs', axis=1, tiled=True)  121 us
    psum x2, waiting for transfers between devices, run_rounds_here(): x_local = lax.psum(x_local, axis_name=k0)  87.8 us
    psum x1, waiting for transfers between devices, local(): summed = lax.psum(partial_grad, 'rep')  63.6 us
    dot_general x1, matrix products, local(): lax.dot_general(columns, lax.all_gather(down_weight, 'fs', axis=1, tiled=...  25.9 us
    reduce_sum x1, other arithmetic, local(): jnp.sum(grad_gate_pre, axis=0)  19.5 us
    dot_general x1, matrix products, local(): lax.dot_general(columns, hidden, (((0,), (0,)), ((), ())), preferred_elem...  15.2 us
  transfers between devices with their start and end apart: 5, of which 5 were waited for; matrix products, arithmetic and copies ran while one was open for 3% of the time, Pallas kernels for 0%

profile of v1, /device:TPU:0, one launch (start us, length us, event | category | flops | bytes accessed | tf_op | source)
XLA Modules:
  0.0 657.4 jit_solution(4270742734075744472)
XLA Ops:
  7.2 0.0 copy-start
  7.2 0.0 all-gather.2.cloned.1.call-start
  7.2 0.7 all-gather.2.cloned.1.call-update
  7.9 0.0 reduce-scatter.2.cloned.1.call-start
  8.0 0.0 copy-start.3
  8.0 5.5 convert_element_type.24
  13.4 0.0 copy-done.3
  13.4 0.0 copy-start.4
  13.4 0.0 copy-start.5
  13.4 0.0 copy-start.7
  13.5 3.4 convert_element_type.23
  16.9 0.0 copy-done.4
  16.9 0.0 copy-done.5
  16.9 120.8 %all-gather.2.cloned.1.call-done = bf16[2048,2048]{1,0:T(8,128)(2,1)} async-done(((bf16[2048,256]{1,0:T(8,128)(2,1)}), bf16[2048,2048]{1,0:T(8,128)(2,1)}) %all-gather.2.cloned.1.call-update) | async-done | bytes 8388624 | tf_op jit(solution)/shard_map/all_gather | solution.py:47
  137.7 0.0 copy-done
  137.7 0.0 copy-done.7
  137.7 0.0 copy-start.1
  137.7 0.0 copy-start.2
  137.7 0.0 copy-start.6
  137.8 25.9 %fusion.4 = (f32[2048]{0:T(1024)}, f32[2048]{0:T(1024)S(1)}, f32[2048]{0:T(1024)S(1)}, f32[2048]{0:T(1024)S(1)}, f32[768,2048]{1,0:T(8,128)}, /*index=5*/f32[768,2048]{1,0:T(8,128)}, f32[768,2048]{1,0:T(8,128)}) fusion(bf16[768,2048]{1,0:T(8,128)(2,1)} %param.9, f32[768,2048]{1,0:T(8,128)} %convert_element_type.23, f32[2048]{0:T(1024)S(1)} %copy-done.7, ...), kind=kOutput, calls=%fused_computation.24 | convolution fusion | flops 6472327168 | bytes 46202880 | tf_op jit(solution)/shard_map/dot_general | solution.py:45
  163.7 0.0 copy-done.1
  163.7 0.0 copy-done.2
  163.7 0.0 copy-done.6
  163.7 19.5 %fusion.5 = (f32[2048]{0:T(1024)}, f32[2048]{0:T(1024)S(1)}, f32[2048]{0:T(1024)S(1)}, f32[2048]{0:T(1024)S(1)}, f32[768,2048]{1,0:T(8,128)}, /*index=5*/f32[768,2048]{1,0:T(8,128)}, bf16[768,2048]{1,0:T(8,128)(2,1)}) fusion(bf16[768,2048]{1,0:T(8,128)(2,1)} %param.8, f32[768,2048]{1,0:T(8,128)S(1)} %copy-done.1, f32[768,2048]{1,0:T(8,128)} %get-tuple-element.30, ...), kind=kLoop, calls=%fused_computation.25 | loop fusion | flops 45604864 | bytes 50397184 | tf_op jit(solution)/shard_map/reduce_sum | solution.py:58
  183.2 15.2 %convolution_bitcast_fusion = f32[2048,2048]{0,1:T(8,128)} fusion(bf16[768,2048]{1,0:T(8,128)(2,1)S(1)} %copy-done, f32[768,2048]{1,0:T(8,128)} %get-tuple-element.32, f32[768,2048]{1,0:T(8,128)} %get-tuple-element.30), kind=kOutput, calls=%fused_computation | convolution fusion | flops 6451888128 | bytes 32505856 | tf_op jit(solution)/shard_map/dot_general | solution.py:74
  198.3 0.0 reduce-scatter.2.cloned.1.call-update
  198.4 0.0 all-reduce.10.cloned.1.call-start
  198.4 278.5 %reduce-scatter.2.cloned.1.call-done = f32[256,2048]{0,1:T(8,128)} async-done(((f32[2048,2048]{0,1:T(8,128)}), f32[256,2048]{0,1:T(8,128)}) %reduce-scatter.2.cloned.1.call-update) | async-done | bytes 2097168 | tf_op jit(solution)/shard_map/reduce_scatter | solution.py:73
  476.9 0.0 all-reduce.10.cloned.1.call-update
  476.9 0.0 all-reduce.14.cloned.1.call-start
  477.0 0.7 pad_maximum_fusion
  477.7 0.0 all-reduce.14.cloned.1.call-update
  477.7 0.0 all-reduce.12.cloned.1.call-start
  477.7 63.6 %all-reduce.10.cloned.1.call-done = f32[2048,256]{1,0:T(8,128)} async-done(((f32[2048,256]{1,0:T(8,128)}), f32[2048,256]{1,0:T(8,128)}) %all-reduce.10.cloned.1.call-update) | async-done | bytes 2097168 | tf_op jit(solution)/shard_map/psum | solution.py:81
  541.3 2.5 multiply_reduce_fusion.6
  543.9 21.5 %all-reduce.14.cloned.1.call-done = (f32[3,2048]{1,0:T(4,128)}, f32[3,2048]{1,0:T(4,128)}, f32[2048]{0:T(1024)}, f32[2048]{0:T(1024)}) async-done(((f32[3,2048]{1,0:T(4,128)}, f32[3,2048]{1,0:T(4,128)}, f32[2048]{0:T(1024)}, f32[2048]{0:T(1024)}), (f32[3,2048]{1,0:T(4,128)}, f32[3,2048]{1,0:T(4,128)}, f32[2048]{0:T(1024)}, f32[2048]{0:T(1024)})) %all-reduce.14.cloned.1.call-update) | async-done | bytes 65552 | tf_op jit(solution)/shard_map/psum | solution.py:66
  565.4 0.0 all-reduce.12.cloned.1.call-update
  565.4 9.4 %add_convert_fusion.1 = bf16[768,2048]{1,0:T(8,128)(2,1)} fusion(f32[768,2048]{1,0:T(8,128)} %get-tuple-element.31, f32[2048]{0:T(1024)S(1)} %bitcast.28, f32[2048]{0:T(1024)S(1)} %bitcast.30, f32[2048]{0:T(1024)S(1)} %bitcast.26), kind=kLoop, calls=%fused_computation.9 | loop fusion | flops 9437184 | bytes 9461760 | tf_op jit(solution)/shard_map/convert_element_type | solution.py:53
  574.8 66.3 %all-reduce.12.cloned.1.call-done = (f32[3,2048]{1,0:T(4,128)}, f32[3,2048]{1,0:T(4,128)}, f32[2048]{0:T(1024)}, f32[2048]{0:T(1024)}, f32[2048]{0:T(1024)}) async-done(((f32[3,2048]{1,0:T(4,128)}, f32[3,2048]{1,0:T(4,128)}, f32[2048]{0:T(1024)}, f32[2048]{0:T(1024)}, f32[2048]{0:T(1024)}), (f32[3,2048]{1,0:T(4,128)}, f32[3,2048]{1,0:T(4,128)}, f32[2048]{0:T(1024)}, f32[2048]{0:T(1024)}, ...) | async-done | bytes 73744 | tf_op jit(solution)/shard_map/psum | solution.py:66
  641.2 1.4 copy.26
  642.5 1.4 copy.27
  643.9 1.3 copy.28
  645.2 1.3 copy.29
  646.5 3.0 copy.30
  649.5 1.3 copy.31
  (2 shorter events, 0.0 us)
Async XLA Ops:
  7.2 130.6 %copy-start = (bf16[768,2048]{1,0:T(8,128)(2,1)S(1)}, bf16[768,2048]{1,0:T(8,128)(2,1)}, u32[]{:S(2)}) copy-start(bf16[768,2048]{1,0:T(8,128)(2,1)} %param.15) | copy-start | bytes 9437188
  7.2 130.5 %all-gather.2.cloned.1.call-start = ((), (), s32[]{:S(2)}) async-start(), calls=%async_computation.1 | async-start | bytes 9437184 | tf_op jit(solution)/shard_map/all_gather | solution.py:47
  7.9 469.0 %reduce-scatter.2.cloned.1.call-start = ((), (), s32[]{:S(2)}) async-start(), calls=%async_computation.2 | async-start | bytes 18874368 | tf_op jit(solution)/shard_map/reduce_scatter | solution.py:73
  8.0 5.5 copy-start.3
  13.4 3.4 copy-start.4
  13.4 3.5 copy-start.5
  13.4 124.3 %copy-start.7 = (f32[2048]{0:T(1024)S(1)}, f32[2048]{0:T(1024)}, u32[]{:S(2)}) copy-start(f32[2048]{0:T(1024)} %param.12) | copy-start | bytes 24580
  137.7 25.9 %copy-start.1 = (f32[768,2048]{1,0:T(8,128)S(1)}, f32[768,2048]{1,0:T(8,128)}, u32[]{:S(2)}) copy-start(f32[768,2048]{1,0:T(8,128)} %convert_element_type.24) | copy-start | bytes 18874372
  137.7 25.9 %copy-start.2 = (f32[768,2048]{1,0:T(8,128)S(1)}, f32[768,2048]{1,0:T(8,128)}, u32[]{:S(2)}) copy-start(f32[768,2048]{1,0:T(8,128)} %convert_element_type.23) | copy-start | bytes 18874372
  137.7 25.9 %copy-start.6 = (f32[2048]{0:T(1024)S(1)}, f32[2048]{0:T(1024)}, u32[]{:S(2)}) copy-start(f32[2048]{0:T(1024)} %param.13) | copy-start | bytes 24580
  198.4 343.0 %all-reduce.10.cloned.1.call-start = ((), (), s32[]{:S(2)}) async-start(), calls=%async_computation.3 | async-start | bytes 4194304 | tf_op jit(solution)/shard_map/psum | solution.py:81
  476.9 88.4 %all-reduce.14.cloned.1.call-start = ((), (), s32[]{:S(2)}) async-start(), calls=%async_computation.5 | async-start | bytes 163840 | tf_op jit(solution)/shard_map/psum | solution.py:66
  477.7 163.5 %all-reduce.12.cloned.1.call-start = ((), (), s32[]{:S(2)}) async-start(), calls=%async_computation.4 | async-start | bytes 180224 | tf_op jit(solution)/shard_map/psum | solution.py:66
Sparse Core Ops, SparseCore 0:
  10.0 127.6 all-gather.1
  198.5 278.3 reduce-scatter.1
  479.2 62.0 all-reduce.9
  544.2 21.1 all-reduce.13
  569.7 71.3 all-reduce.11
